TPU v7x, 32 devices: a whole 2x2x4 slice. The times are simulated.
32 devices in a mesh: fs: 8 (over z, x), tp: 4 (over y, core).
Axes of the slice: x: 2, y: 2, z: 4, core: 2. Of those that a mesh axis runs over, the one named last changes fastest.
Arguments:
- x_late: bfloat16 [4096, 2048], P(('fs', 'tp')), may hold values from -6 to 6
- x_early: bfloat16 [4096, 2048], P(('fs', 'tp')), may hold values from -6 to 6
- d_hidden: bfloat16 [4096, 3072], P('fs', 'tp'), may hold values from -6 to 6
- w_gate: bfloat16 [2048, 3072], P('fs', 'tp'), may hold values from -0.125 to 0.125
- w_up: bfloat16 [2048, 3072], P('fs', 'tp'), may hold values from -0.125 to 0.125
- gate_sum: float32 [2048, 3072], P('fs', 'tp'), may hold values from -192 to 192
- up_sum: float32 [2048, 3072], P('fs', 'tp'), may hold values from -192 to 192
Outputs:
- hidden_late: bfloat16 [4096, 3072], P('fs', 'tp')
- grad_input: bfloat16 [4096, 2048], P(('fs', 'tp'))
- gate_sum_out: float32 [2048, 3072], P('fs', 'tp')
- up_sum_out: float32 [2048, 3072], P('fs', 'tp')
All inputs are finite; a program needn't handle non-finite values.
Results may differ from a plain program's by a relative error of at most 0.0095.
Values may be sent and summed in bfloat16 or wider, within the bound.
A program may use at most 128 MiB of HBM per device.

v0:
```python
import jax
import jax.numpy as jnp
from jax import lax
from jax.sharding import PartitionSpec as P


def local(x_late, x_early, d_hidden, w_gate, w_up, gate_sum, up_sum):
    rows_late, rows_early = (
        lax.all_gather(x_late, "tp", axis=0, tiled=True),
        lax.all_gather(x_early, "tp", axis=0, tiled=True),
    )
    stacked = jnp.concatenate([rows_late, rows_early], axis=0)
    row_count = rows_late.shape[0]
    col_count = w_gate.shape[1]
    contract = (((1,), (1,)), ((), ()))
    tokens_dim = (((0,), (0,)), ((), ()))
    full_gate, full_up = (
        lax.all_gather(w_gate, "fs", axis=0, tiled=True),
        lax.all_gather(w_up, "fs", axis=0, tiled=True),
    )
    gate_pre = jnp.dot(stacked, full_gate, preferred_element_type=jnp.float32)
    up_pre = jnp.dot(stacked, full_up, preferred_element_type=jnp.float32)
    sigmoid_all = jax.nn.sigmoid(gate_pre)
    hidden_late = (gate_pre[:row_count] * sigmoid_all[:row_count] * up_pre[:row_count]).astype(
        jnp.bfloat16
    )
    gate_early = gate_pre[row_count:]
    up_early = up_pre[row_count:]
    sigmoid_early = sigmoid_all[row_count:]
    cotangent = d_hidden.astype(jnp.float32)
    d_gate = (
        cotangent * up_early * sigmoid_early * (1.0 + gate_early * (1.0 - sigmoid_early))
    ).astype(jnp.bfloat16)
    d_up = (cotangent * gate_early * sigmoid_early).astype(jnp.bfloat16)
    full_gate, full_up = (
        lax.all_gather(w_gate, "fs", axis=0, tiled=True),
        lax.all_gather(w_up, "fs", axis=0, tiled=True),
    )
    partial_value = lax.dot_general(d_gate, full_gate, contract, preferred_element_type=jnp.float32)
    partial_value = partial_value + lax.dot_general(
        d_up, full_up, contract, preferred_element_type=jnp.float32
    )
    rounded = lax.optimization_barrier(partial_value.astype(jnp.bfloat16)).astype(jnp.float32)
    grad_input = lax.psum_scatter(
        rounded.astype(jnp.bfloat16), "tp", scatter_dimension=0, tiled=True
    )
    d_both = jnp.concatenate([d_gate, d_up], axis=1)
    gradient = lax.psum_scatter(
        lax.dot_general(rows_early, d_both, tokens_dim, preferred_element_type=jnp.float32),
        "fs",
        scatter_dimension=0,
        tiled=True,
    )
    gate_grad = gradient[:, :col_count]
    up_grad = gradient[:, col_count:]
    return (hidden_late, grad_input, gate_sum + gate_grad, up_sum + up_grad)


def solution(mesh):
    return jax.shard_map(
        local,
        mesh=mesh,
        in_specs=(
            P(("fs", "tp"), None),
            P(("fs", "tp"), None),
            P("fs", "tp"),
            P("fs", "tp"),
            P("fs", "tp"),
            P("fs", "tp"),
            P("fs", "tp"),
        ),
        out_specs=(P("fs", "tp"), P(("fs", "tp"), None), P("fs", "tp"), P("fs", "tp")),
        check_vma=False,
    )
```

profile of v0, /device:TPU:0, one launch (start us, length us, event | category | flops | bytes accessed | tf_op | source)
XLA Modules:
  0.0 444.5 jit_solution(2437390154084360993)
XLA Ops:
  7.2 0.0 all-gather.5.cloned.1.call-start
  7.2 0.7 all-gather.5.cloned.1.call-update
  7.9 0.0 all-gather.7.cloned.1.call-start
  7.9 0.7 all-gather.7.cloned.1.call-update
  8.6 0.0 all-gather.11.cloned.1.call-start
  8.7 0.7 all-gather.11.cloned.1.call-update
  9.4 0.0 all-gather.9.cloned.1.call-start
  9.4 0.5 all-gather.9.cloned.1.call-update
  10.0 0.0 reduce-scatter.5.cloned.1.call-start
  10.0 1.4 copy.11
  11.4 23.4 %all-gather.5.cloned.1.call-done = bf16[512,2048]{1,0:T(8,128)(2,1)} async-done(((bf16[128,2048]{1,0:T(8,128)(2,1)}), bf16[512,2048]{1,0:T(8,128)(2,1)}) %all-gather.5.cloned.1.call-update) | async-done | bytes 2097168 | tf_op jit(solution)/shard_map/all_gather | solution.py:9
  34.9 3.2 constant_dynamic-update-slice_fusion.1
  38.0 21.0 %all-gather.7.cloned.1.call-done = bf16[512,2048]{1,0:T(8,128)(2,1)} async-done(((bf16[128,2048]{1,0:T(8,128)(2,1)}), bf16[512,2048]{1,0:T(8,128)(2,1)}) %all-gather.7.cloned.1.call-update) | async-done | bytes 2097168 | tf_op jit(solution)/shard_map/all_gather | solution.py:10
  59.0 3.2 constant_dynamic-update-slice_fusion
  62.2 59.1 %all-gather.11.cloned.1.call-done = bf16[2048,768]{1,0:T(8,128)(2,1)} async-done(((bf16[256,768]{1,0:T(8,128)(2,1)}), bf16[2048,768]{1,0:T(8,128)(2,1)}) %all-gather.11.cloned.1.call-update) | async-done | bytes 3145744 | tf_op jit(solution)/shard_map/all_gather | solution.py:19
  121.2 8.3 %fusion.10 = f32[1024,768]{0,1:T(8,128)} fusion(bf16[1024,2048]{1,0:T(8,128)(2,1)} %constant_dynamic-update-slice_fusion, bf16[2048,768]{1,0:T(8,128)(2,1)} %all-gather.11.cloned.1.call-done), kind=kOutput, calls=%fused_computation.21 | convolution fusion | flops 3221225472 | bytes 10485760 | tf_op jit(solution)/shard_map/dot_general | solution.py:22
  129.6 52.4 %all-gather.9.cloned.1.call-done = bf16[2048,768]{1,0:T(8,128)(2,1)} async-done(((bf16[256,768]{1,0:T(8,128)(2,1)}), bf16[2048,768]{1,0:T(8,128)(2,1)}) %all-gather.9.cloned.1.call-update) | async-done | bytes 3145744 | tf_op jit(solution)/shard_map/all_gather | solution.py:18
  182.0 0.0 copy-start
  182.0 6.8 %add_divide_fusion = (f32[1024,768]{0,1:T(8,128)S(1)}, f32[1024,768]{0,1:T(8,128)S(1)}) fusion(bf16[1024,2048]{1,0:T(8,128)(2,1)} %constant_dynamic-update-slice_fusion, bf16[2048,768]{1,0:T(8,128)(2,1)} %all-gather.9.cloned.1.call-done), kind=kOutput, calls=%fused_computation.2 | convolution fusion | flops 3223584768 | bytes 13631488 | tf_op jit(solution)/shard_map/dot_general | solution.py:21
  188.8 0.0 copy-done
  188.8 0.0 copy-start.1
  188.8 1.4 fusion.2
  190.3 0.1 copy-done.1
  190.4 7.3 %convolution_bitcast_fusion = f32[2048,1536]{0,1:T(8,128)} fusion(bf16[512,2048]{1,0:T(8,128)(2,1)S(1)} %copy-done.1, bf16[512,768]{0,1:T(8,128)(2,1)S(1)} %get-tuple-element.10, bf16[512,768]{0,1:T(8,128)(2,1)S(1)} %get-tuple-element.8), kind=kOutput, calls=%fused_computation | convolution fusion | flops 3224371200 | bytes 16252928 | tf_op jit(solution)/shard_map/dot_general | solution.py:49
  197.7 0.0 reduce-scatter.5.cloned.1.call-update
  197.8 0.2 reduce-scatter.3.cloned.1.call-start
  198.0 0.0 copy-start.3
  198.0 3.9 fusion.11
  201.9 0.0 copy-done.3
  201.9 0.0 copy-start.2
  201.9 3.2 add_convert_fusion
  205.1 0.0 reduce-scatter.3.cloned.1.call-update
  205.2 0.0 copy-done.2
  205.2 0.3 copy.13
  205.5 1.4 copy.12
  206.9 1.2 copy.14
  208.0 196.4 %reduce-scatter.5.cloned.1.call-done = f32[256,1536]{0,1:T(8,128)} async-done(((f32[2048,1536]{0,1:T(8,128)}), f32[256,1536]{0,1:T(8,128)}) %reduce-scatter.5.cloned.1.call-update) | async-done | bytes 1572880 | tf_op jit(solution)/shard_map/reduce_scatter | solution.py:48
  404.4 1.6 slice_add_fusion
  406.0 1.1 copy.15
  407.1 1.1 copy.16
  408.3 29.4 %reduce-scatter.3.cloned.1.call-done = bf16[128,2048]{1,0:T(8,128)(2,1)} async-done(((bf16[512,2048]{1,0:T(8,128)(2,1)}), bf16[128,2048]{1,0:T(8,128)(2,1)}) %reduce-scatter.3.cloned.1.call-update) | async-done | bytes 524304 | tf_op jit(solution)/shard_map/reduce_scatter | solution.py:44
Async XLA Ops:
  7.2 27.7 %all-gather.5.cloned.1.call-start = ((), (), s32[]{:S(2)}) async-start(), calls=%async_computation.2 | async-start | bytes 2621440 | tf_op jit(solution)/shard_map/all_gather | solution.py:9
  7.9 51.1 %all-gather.7.cloned.1.call-start = ((), (), s32[]{:S(2)}) async-start(), calls=%async_computation.3 | async-start | bytes 2621440 | tf_op jit(solution)/shard_map/all_gather | solution.py:10
  8.6 112.6 %all-gather.11.cloned.1.call-start = ((), (), s32[]{:S(2)}) async-start(), calls=%async_computation.5 | async-start | bytes 3538944 | tf_op jit(solution)/shard_map/all_gather | solution.py:19
  9.4 172.6 %all-gather.9.cloned.1.call-start = ((), (), s32[]{:S(2)}) async-start(), calls=%async_computation.4 | async-start | bytes 3538944 | tf_op jit(solution)/shard_map/all_gather | solution.py:18
  10.0 394.5 %reduce-scatter.5.cloned.1.call-start = ((), (), s32[]{:S(2)}) async-start(), calls=%async_computation.7 | async-start | bytes 14155776 | tf_op jit(solution)/shard_map/reduce_scatter | solution.py:48
  182.0 6.8 %copy-start = (f32[1024,768]{0,1:T(8,128)S(1)}, f32[1024,768]{0,1:T(8,128)}, u32[]{:S(2)}) copy-start(f32[1024,768]{0,1:T(8,128)} %fusion.10) | copy-start | bytes 9437188
  188.8 1.6 copy-start.1
  197.8 239.9 %reduce-scatter.3.cloned.1.call-start = ((), (), s32[]{:S(2)}) async-start(), calls=%async_computation.6 | async-start | bytes 2621440 | tf_op jit(solution)/shard_map/reduce_scatter | solution.py:44
  198.0 3.9 copy-start.3
  201.9 3.3 copy-start.2
Sparse Core Ops, SparseCore 0:
  9.5 25.2 all-gather.4
  36.4 22.5 all-gather.6
  61.2 59.9 all-gather.10
  123.3 58.6 all-gather.8
  197.9 206.5 reduce-scatter.4
  407.4 30.2 reduce-scatter.2
where the time goes:
time: 445 us
  waiting for transfers between devices  384 us (86%)
  matrix products  29.6 us (7%)
  between operations  14.2 us (3%)
  local copies, waits for them, and re-layouts  13 us (3%)
    reduce_scatter x1, waiting for transfers between devices, local(): lax.psum_scatter(lax.dot_general(rows_early, d_both, tokens_dim, preferre...  196 us
    all_gather x1, waiting for transfers between devices, local(): lax.all_gather(w_up, 'fs', axis=0, tiled=True)  59.1 us
    all_gather x1, waiting for transfers between devices, local(): lax.all_gather(w_gate, 'fs', axis=0, tiled=True)  52.4 us
    reduce_scatter x1, waiting for transfers between devices, local(): lax.psum_scatter(rounded.astype(jnp.bfloat16), 'tp', scatter_dimension=0,...  29.4 us
    all_gather x1, waiting for transfers between devices, local(): lax.all_gather(x_late, 'tp', axis=0, tiled=True)  23.4 us
    all_gather x1, waiting for transfers between devices, local(): lax.all_gather(x_early, 'tp', axis=0, tiled=True)  21 us
    unnamed x15, local copies, waits for them, and re-layouts  9.85 us
  transfers between devices with their start and end apart: 6, of which 6 were waited for; matrix products, arithmetic and copies ran while one was open for 7% of the time, Pallas kernels for 0%

commit v1 on v0

v1 whole, which is shorter than its diff:
```python
import functools

import jax
import jax.numpy as jnp
from jax import lax
from jax.experimental import pallas as pl
from jax.experimental.pallas import tpu as pltpu
from jax.sharding import PartitionSpec as P

MESH = pl.DeviceIdType.MESH
F32 = jnp.float32
BF16 = jnp.bfloat16


def place(fs_count):
    fs, tp = lax.axis_index("fs"), lax.axis_index("tp")
    return lax.div(fs, 2), lax.rem(fs, 2), tp, fs_count // 2


def greet(devices):
    barrier = pltpu.get_barrier_semaphore()
    for device in devices:
        pl.semaphore_signal(barrier, inc=1, device_id=device, device_id_type=MESH)
    pl.semaphore_wait(barrier, len(devices))


def bits_of(tp_count):
    return [1 << b for b in range(tp_count.bit_length() - 1)]


def flip(tp, bit):
    return jnp.where(lax.rem(lax.div(tp, bit), 2) == 0, tp + bit, tp - bit)


def flips(tp, mask, bits):
    for bit in bits:
        if mask & bit:
            tp = flip(tp, bit)
    return tp


class Copies:
    def __init__(self, send_sem, recv_sem):
        self.send_sem, self.recv_sem = send_sem, recv_sem
        self.made, self.waited = {}, set()

    def start(self, key, src, dst, device):
        index = len(self.made)
        copy = pltpu.make_async_remote_copy(
            src_ref=src,
            dst_ref=dst,
            send_sem=self.send_sem.at[index],
            recv_sem=self.recv_sem.at[index],
            device_id=device,
            device_id_type=MESH,
        )
        copy.start()
        self.made[key] = copy

    def arrived(self, key):
        if key not in self.waited:
            self.waited.add(key)
            self.made[key].wait_recv()

    def drain(self):
        for copy in self.made.values():
            copy.wait_send()


def gather_kernel(fs_count, tp_count, xl, xe, wg, wu, out_xl, out_xe, out_wg, out_wu, ssem, rsem):
    z, x, tp, n = place(fs_count)
    bits = bits_of(tp_count)
    rows, half = wg.shape[0], wg.shape[1] // 2
    tokens = xl.shape[0]
    ahead = (lax.rem(z + 1, n) * 2 + x, tp)
    behind = (lax.rem(z + n - 1, n) * 2 + x, tp)
    beside = (z * 2 + 1 - x, tp)
    greet([ahead, behind, beside] + [(z * 2 + x, flip(tp, bit)) for bit in bits])
    copies = Copies(ssem, rsem)

    def block(offset, side):
        at = lax.rem(z + offset + n, n) * 2 + side
        return pl.ds(pl.multiple_of(at * rows, rows), rows)

    def own_tokens(mask):
        return pl.ds(pl.multiple_of(flips(tp, mask, bits) * tokens, tokens), tokens)

    lanes = {"f": pl.ds(0, half), "b": pl.ds(half, half)}
    towards = {"f": ahead, "b": behind}
    mine = block(0, x)
    for name, src, out in (("e", xe, out_xe), ("l", xl, out_xl)):
        for bit in bits[::-1]:
            copies.start((name, bit, 0), src, out.at[own_tokens(0)], (z * 2 + x, flip(tp, bit)))
    for way in "fb":
        copies.start(("up", way, 0), wu.at[:, lanes[way]], out_wu.at[mine, lanes[way]], towards[way])
    copies.start("gate_beside", wg, out_wg.at[mine], beside)
    for way in "fb":
        copies.start(("gate", way, 0), wg.at[:, lanes[way]], out_wg.at[mine, lanes[way]], towards[way])
    copies.start("up_beside", wu, out_wu.at[mine], beside)
    out_wu[mine, :] = wu[...]
    out_wg[mine, :] = wg[...]
    out_xe[own_tokens(0), :] = xe[...]
    out_xl[own_tokens(0), :] = xl[...]

    def ring(name, out, side, way, step):
        copies.arrived((name, way, step))
        offset = -1 - step if way == "f" else 1 + step
        at = (block(offset, side), lanes[way])
        if step < n - 2:
            copies.start((name, way, step + 1), out.at[at], out.at[at], towards[way])
        return at

    def spread(step):
        for way in "fb":
            at = ring("up", out_wu, x, way, step)
            copies.start(("up_beside", way, step), out_wu.at[at], out_wu.at[at], beside)

    spread(0)
    copies.arrived("gate_beside")
    other = block(0, 1 - x)
    for way in "fb":
        at = (other, lanes[way])
        copies.start(("pair", way, 0), out_wg.at[at], out_wg.at[at], towards[way])
    for step in range(n - 1):
        if step:
            spread(step)
        for way in "fb":
            ring("gate", out_wg, x, way, step)
        if step == 0:
            for place_of, bit in enumerate(bits[::-1]):
                held = bits[::-1][:place_of]
                for mask in range(1, tp_count):
                    if any(mask & b for b in bits if b not in held):
                        continue
                    for name, out in (("e", out_xe), ("l", out_xl)):
                        top = mask & -mask
                        copies.arrived((name, top, mask ^ top))
                        at = own_tokens(mask)
                        copies.start((name, bit, mask), out.at[at], out.at[at], (z * 2 + x, flip(tp, bit)))
        for way in "fb":
            ring("pair", out_wg, 1 - x, way, step)
    copies.arrived("up_beside")
    for step in range(n - 1):
        for way in "fb":
            copies.arrived(("up_beside", way, step))
    for name in "el":
        for mask in range(1, tp_count):
            low = mask & -mask
            copies.arrived((name, low, mask ^ low))
    copies.drain()


def add(a, b):
    return a.astype(F32) + b.astype(F32)


def reduce_kernel(
    fs_count, tp_count, dg, du, dx, gs, us, out_g, out_u, out_x,
    slots_a, last_a, slots_b, slots_c, slots_x, ssem, rsem,
):
    z, x, tp, n = place(fs_count)
    bits = bits_of(tp_count)
    rows, half = gs.shape[0], gs.shape[1] // 2
    tokens = out_x.shape[0]
    ahead = (lax.rem(z + 1, n) * 2 + x, tp)
    behind = (lax.rem(z + n - 1, n) * 2 + x, tp)
    beside = (z * 2 + 1 - x, tp)
    greet([ahead, behind, beside] + [(z * 2 + x, flip(tp, bit)) for bit in bits])
    copies = Copies(ssem, rsem)
    lanes = {"f": pl.ds(0, half), "b": pl.ds(half, half)}
    towards = {"f": ahead, "b": behind}

    def pair(offset):
        at = lax.rem(z + offset + n, n)
        return pl.ds(pl.multiple_of(at * 2 * rows, 2 * rows), 2 * rows)

    def block(offset, side):
        at = lax.rem(z + offset + n, n) * 2 + side
        return pl.ds(pl.multiple_of(at * rows, rows), rows)

    def chunk(mask):
        return pl.ds(pl.multiple_of(flips(tp, mask, bits) * tokens, tokens), tokens)

    for way in "fb":
        at = (pair(-1 if way == "f" else 1), lanes[way])
        copies.start(("a", way, 0), dg.at[at], slots_a.at[0, :, lanes[way]], towards[way])
    order = []
    for step in range(n):
        for offset in ((-1 - step) % n, (1 + step) % n):
            if offset not in order:
                order.append(offset)
    for offset in order:
        copies.start(("b", offset), du.at[block(offset, 1 - x)], slots_b.at[offset], beside)

    def above(bit):
        return [m for m in range(0, tp_count, 2 * bit)]

    slot_of = {}
    for bit in bits:
        for mask in above(bit):
            slot_of[bit, mask] = len(slot_of)
    first = bits[0]
    for mask in above(first)[::-1]:
        copies.start(("x", first, mask), dx.at[chunk(mask | first)], slots_x.at[slot_of[first, mask]], (z * 2 + x, flip(tp, first)))

    def sum_x(bit, mask):
        total = dx[chunk(mask), :].astype(F32)
        for b in bits:
            if b <= bit:
                total = total + slots_x[slot_of[b, mask]].astype(F32)
        return total

    for level in range(1, len(bits)):
        bit = bits[level]
        for mask in above(bit)[::-1]:
            sent = mask | bit
            for b in bits[:level]:
                if b == bits[level - 1]:
                    copies.arrived(("x", b, sent))
            slot = slots_x.at[slot_of[bits[level - 1], sent]]
            slot[...] = sum_x(bits[level - 1], sent).astype(BF16)
            copies.start(("x", bit, mask), slot, slots_x.at[slot_of[bit, mask]], (z * 2 + x, flip(tp, bit)))

    ready = set()

    def beside_sum(offset):
        offset = offset % n
        if offset not in ready:
            ready.add(offset)
            copies.arrived(("b", offset))
            if offset:
                slots_b[offset] = add(slots_b[offset], du[block(offset, x), :]).astype(BF16)
        return offset

    for way in "fb":
        offset = beside_sum(-1 if way == "f" else 1)
        copies.start(("c", way, 0), slots_b.at[offset, :, lanes[way]], slots_c.at[0, :, lanes[way]], towards[way])
    for step in range(n - 1):
        for way in "fb":
            copies.arrived(("a", way, step))
            if step < n - 2:
                at = (pair(-2 - step if way == "f" else 2 + step), lanes[way])
                slots_a[step, :, lanes[way]] = add(slots_a[step, :, lanes[way]], dg[at]).astype(BF16)
                copies.start(("a", way, step + 1), slots_a.at[step, :, lanes[way]], slots_a.at[step + 1, :, lanes[way]], towards[way])
            else:
                there = pl.ds(pl.multiple_of((1 - x) * rows, rows), rows)
                at = (there, lanes[way])
                slots_a[step, there, lanes[way]] = add(
                    slots_a[step, there, lanes[way]], dg[block(0, 1 - x), lanes[way]]
                ).astype(BF16)
                copies.start(("last", way), slots_a.at[step, there, lanes[way]], last_a.at[:, lanes[way]], beside)
        for way in "fb":
            offset = beside_sum(-2 - step if way == "f" else 2 + step)
            copies.arrived(("c", way, step))
            if step < n - 2:
                slots_c[step, :, lanes[way]] = add(
                    slots_c[step, :, lanes[way]], slots_b[offset, :, lanes[way]]
                ).astype(BF16)
                copies.start(("c", way, step + 1), slots_c.at[step, :, lanes[way]], slots_c.at[step + 1, :, lanes[way]], towards[way])
    for b in bits:
        copies.arrived(("x", b, 0))
    out_x[...] = sum_x(bits[-1], 0).astype(BF16)
    out_u[...] = us[...] + (
        add(slots_b[0], du[block(0, x), :]) + slots_c[n - 2].astype(F32)
    )
    here = pl.ds(pl.multiple_of(x * rows, rows), rows)
    for way in "fb":
        copies.arrived(("last", way))
    out_g[...] = gs[...] + (
        add(slots_a[n - 2, here, :], dg[block(0, x), :]) + last_a[...].astype(F32)
    )
    copies.drain()


def vmem(count):
    return [pl.BlockSpec(memory_space=pltpu.VMEM)] * count


def local(fs_count, tp_count, x_late, x_early, d_hidden, w_gate, w_up, gate_sum, up_sum):
    n = fs_count // 2
    tokens, width = x_early.shape
    rows, cols = w_gate.shape
    full = jax.ShapeDtypeStruct((fs_count * rows, cols), BF16)
    group = jax.ShapeDtypeStruct((tp_count * tokens, width), BF16)
    count = 2 * (tp_count - 1) + 8 * (n - 1) + 2
    rows_late, rows_early, full_gate, full_up = pl.pallas_call(
        functools.partial(gather_kernel, fs_count, tp_count),
        out_shape=(group, group, full, full),
        in_specs=vmem(4),
        out_specs=tuple(vmem(4)),
        scratch_shapes=[pltpu.SemaphoreType.DMA((count,)), pltpu.SemaphoreType.DMA((count,))],
        compiler_params=pltpu.CompilerParams(collective_id=0, has_side_effects=True),
        name="gather",
    )(x_late, x_early, w_gate, w_up)

    contract = (((1,), (1,)), ((), ()))
    tokens_dim = (((0,), (0,)), ((), ()))
    gate_early = jnp.dot(rows_early, full_gate, preferred_element_type=F32)
    up_early = jnp.dot(rows_early, full_up, preferred_element_type=F32)
    s = jax.nn.sigmoid(gate_early)
    cotangent = d_hidden.astype(F32)
    d_gate = (cotangent * up_early * s * (1.0 + gate_early * (1.0 - s))).astype(BF16)
    d_up = (cotangent * gate_early * s).astype(BF16)
    grad_gate = lax.dot_general(rows_early, d_gate, tokens_dim, preferred_element_type=F32).astype(BF16)
    grad_up = lax.dot_general(rows_early, d_up, tokens_dim, preferred_element_type=F32).astype(BF16)
    partial_value = lax.dot_general(d_gate, full_gate, contract, preferred_element_type=F32)
    partial_value = partial_value + lax.dot_general(d_up, full_up, contract, preferred_element_type=F32)
    partial_value = partial_value.astype(BF16)
    gate_late = jnp.dot(rows_late, full_gate, preferred_element_type=F32)
    up_late = jnp.dot(rows_late, full_up, preferred_element_type=F32)
    hidden_late = (gate_late * jax.nn.sigmoid(gate_late) * up_late).astype(BF16)

    count = (tp_count - 1) + 4 * (n - 1) + n + 2
    gate_out, up_out, grad_input = pl.pallas_call(
        functools.partial(reduce_kernel, fs_count, tp_count),
        out_shape=(
            jax.ShapeDtypeStruct(gate_sum.shape, F32),
            jax.ShapeDtypeStruct(up_sum.shape, F32),
            jax.ShapeDtypeStruct(x_early.shape, BF16),
        ),
        in_specs=vmem(5),
        out_specs=tuple(vmem(3)),
        scratch_shapes=[
            pltpu.VMEM((n - 1, 2 * rows, cols), BF16),
            pltpu.VMEM((rows, cols), BF16),
            pltpu.VMEM((n, rows, cols), BF16),
            pltpu.VMEM((n - 1, rows, cols), BF16),
            pltpu.VMEM((tp_count - 1, tokens, width), BF16),
            pltpu.SemaphoreType.DMA((count,)),
            pltpu.SemaphoreType.DMA((count,)),
        ],
        compiler_params=pltpu.CompilerParams(collective_id=1, has_side_effects=True),
        name="reduce",
    )(grad_gate, grad_up, partial_value, gate_sum, up_sum)
    return (hidden_late, grad_input, gate_out, up_out)


def solution(mesh):
    return jax.shard_map(
        functools.partial(local, mesh.shape["fs"], mesh.shape["tp"]),
        mesh=mesh,
        in_specs=(
            P(("fs", "tp"), None),
            P(("fs", "tp"), None),
            P("fs", "tp"),
            P("fs", "tp"),
            P("fs", "tp"),
            P("fs", "tp"),
            P("fs", "tp"),
        ),
        out_specs=(P("fs", "tp"), P(("fs", "tp"), None), P("fs", "tp"), P("fs", "tp")),
        check_vma=False,
    )
```

time: 445 us -> 203 us (0.46)
  waiting for transfers between devices: 384 us -> 0 us
  Pallas kernels: 0 us -> 173 us
  between operations: 14.2 us -> 0.76 us
  local copies, waits for them, and re-layouts: 13 us -> 5.32 us
  matrix products: 29.6 us -> 23.6 us
    reduce_scatter x2 -> x0, waiting for transfers between devices: 226 us -> none  [the longest x1 196 us: local(): lax.psum_scatter(lax.dot_general(rows_early, d_both, tokens_dim, preferre...]
    pallas_call x0 -> x2, Pallas kernels: none -> 173 us  [the longest x1 87.2 us: local(): pl.pallas_call(functools.partial(gather_kernel, fs_count, tp_count), out_...]
    all_gather x4 -> x0, waiting for transfers between devices: 156 us -> none  [the longest x1 59.1 us: local(): lax.all_gather(w_up, 'fs', axis=0, tiled=True)]
    dot_general x5 -> x8, matrix products: 29.6 us -> 23.6 us  [the longest x1 4.45 us: local(): gate_early = jnp.dot(rows_early, full_gate, preferred_element_type=F32)]
    unnamed x15, local copies, waits for them, and re-layouts: 9.85 us -> 5.32 us
  transfers between devices with their start and end apart: 6 -> 0, of which waited for: 6 -> 0; matrix products, arithmetic and copies ran while one was open for 7% -> 0% of each run, Pallas kernels for 0% -> 0%
where the time goes in v1:
time: 203 us
  Pallas kernels  173 us (85%)
  matrix products  23.6 us (12%)
  local copies, waits for them, and re-layouts  5.32 us (3%)
    pallas_call x1, Pallas kernels, local(): pl.pallas_call(functools.partial(gather_kernel, fs_count, tp_count), out_...  87.2 us
    pallas_call x1, Pallas kernels, local(): pl.pallas_call(functools.partial(reduce_kernel, fs_count, tp_count), out_...  85.7 us
    unnamed x15, local copies, waits for them, and re-layouts  5.32 us
    dot_general x1, matrix products, local(): gate_early = jnp.dot(rows_early, full_gate, preferred_element_type=F32)  4.45 us

profile of v1, /device:TPU:0, one launch (start us, length us, event | category | flops | bytes accessed | tf_op | source)
XLA Modules:
  0.0 202.5 jit_solution(14183063515540589881)
XLA Ops:
  0.6 87.2 %gather.1 = (bf16[512,2048]{1,0:T(8,128)(2,1)}, bf16[512,2048]{1,0:T(8,128)(2,1)}, bf16[2048,768]{1,0:T(8,128)(2,1)}, bf16[2048,768]{1,0:T(8,128)(2,1)}) custom-call(bf16[128,2048]{1,0:T(8,128)(2,1)} %xl.1, bf16[128,2048]{1,0:T(8,128)(2,1)} %xe.1, bf16[256,768]{1,0:T(8,128)(2,1)} %wg.1, bf16[256,768]{1,0:T(8,128)(2,1)} %wu.1), custom_call_target="tpu_custom_call" | custom-call | tf_op jit(solution)/shard_map/gather/pallas_call | solution.py:286
  87.8 0.0 copy-start.1
  87.8 0.0 copy-start.3
  87.8 0.0 copy-start.5
  87.8 4.5 %fusion.8 = f32[512,768]{1,0:T(8,128)S(1)} fusion(bf16[512,2048]{1,0:T(8,128)(2,1)} %get-tuple-element.14, bf16[2048,768]{1,0:T(8,128)(2,1)} %get-tuple-element.12), kind=kOutput, calls=%fused_computation.13 | convolution fusion | flops 1610612736 | bytes 6815744 | tf_op jit(solution)/shard_map/dot_general | solution.py:298
  92.3 0.0 copy-done.1
  92.3 0.0 copy-done.3
  92.3 0.0 copy-done.5
  92.3 0.0 copy-start.2
  92.3 0.0 copy-start.4
  92.3 2.1 %fusion.2 = bf16[512,768]{1,0:T(8,128)(2,1)S(1)} fusion(bf16[512,768]{1,0:T(8,128)(2,1)S(1)} %copy-done.5, f32[512,768]{1,0:T(8,128)S(1)} %fusion.8, bf16[512,2048]{1,0:T(8,128)(2,1)S(1)} %copy-done.3, bf16[2048,768]{1,0:T(8,128)(2,1)S(1)} %copy-done.1), kind=kOutput, calls=%fused_computation.7 | convolution fusion | flops 1614938112 | bytes 8388608 | tf_op jit(solution)/shard_map/dot_general | solution.py:299
  94.4 0.0 copy-done.2
  94.5 0.4 copy-done.4
  94.9 1.8 fusion.7
  96.7 2.8 %multiply_convert_fusion = bf16[512,768]{1,0:T(8,128)(2,1)} fusion(f32[512,768]{1,0:T(8,128)S(1)} %fusion.7, bf16[512,2048]{1,0:T(8,128)(2,1)S(1)} %copy-done.4, bf16[2048,768]{1,0:T(8,128)(2,1)S(1)} %copy-done.1), kind=kOutput, calls=%fused_computation.11 | convolution fusion | flops 1612972032 | bytes 7602176 | tf_op jit(solution)/shard_map/dot_general | solution.py:310
  99.5 1.8 fusion.9
  101.3 3.2 %add_convert_fusion.dx = bf16[512,2048]{1,0:T(8,128)(2,1)} fusion(f32[512,2048]{1,0:T(8,128)S(1)} %fusion.9, bf16[2048,768]{1,0:T(8,128)(2,1)S(1)} %copy-done.1, f32[512,768]{1,0:T(8,128)S(1)} %fusion.8, bf16[512,768]{1,0:T(8,128)(2,1)S(1)} %copy-done.5), kind=kOutput, calls=%fused_computation | convolution fusion | flops 1615462400 | bytes 11796480 | tf_op jit(solution)/shard_map/dot_general | solution.py:307
  104.5 3.6 %convolution_convert_fusion.du = bf16[2048,768]{1,0:T(8,128)(2,1)} fusion(bf16[512,2048]{1,0:T(8,128)(2,1)S(1)} %copy-done.3, f32[512,768]{1,0:T(8,128)S(1)} %fusion.8, bf16[512,768]{1,0:T(8,128)(2,1)S(1)} %copy-done.5), kind=kOutput, calls=%fused_computation.1 | convolution fusion | flops 1614938112 | bytes 7602176 | tf_op jit(solution)/shard_map/dot_general | solution.py:305
  108.2 3.7 %convolution_convert_fusion.1.dg = bf16[2048,768]{1,0:T(8,128)(2,1)} fusion(bf16[512,2048]{1,0:T(8,128)(2,1)S(1)} %copy-done.3, bf16[512,768]{1,0:T(8,128)(2,1)S(1)} %fusion.2), kind=kOutput, calls=%fused_computation.2 | convolution fusion | flops 1612185600 | bytes 6029312 | tf_op jit(solution)/shard_map/dot_general | solution.py:304
  111.9 85.7 %reduce.1 = (f32[256,768]{1,0:T(8,128)}, f32[256,768]{1,0:T(8,128)}, bf16[128,2048]{1,0:T(8,128)(2,1)}) custom-call(bf16[2048,768]{1,0:T(8,128)(2,1)} %convolution_convert_fusion.1.dg, bf16[2048,768]{1,0:T(8,128)(2,1)} %convolution_convert_fusion.du, bf16[512,2048]{1,0:T(8,128)(2,1)} %add_convert_fusion.dx, f32[256,768]{1,0:T(8,128)} %gs.1, f32[256,768]{1,0:T(8,128)} %us.1), custom_call_target="tpu_custom_call" | custom-call | tf_op jit(solution)/shard_map/reduce/pallas_call | solution.py:314
  197.6 0.0 copy-start
  197.6 2.0 copy.14
  199.6 2.1 %copy.15 = f32[256,768]{1,0:T(8,128)} copy(f32[256,768]{1,0:T(8,128)} %get-tuple-element.24) | data formatting | bytes 1572864
  201.6 0.0 copy-done
  201.6 0.9 copy.16
Async XLA Ops:
  87.8 4.5 %copy-start.1 = (bf16[2048,768]{1,0:T(8,128)(2,1)S(1)}, bf16[2048,768]{1,0:T(8,128)(2,1)}, u32[]{:S(2)}) copy-start(bf16[2048,768]{1,0:T(8,128)(2,1)} %get-tuple-element.13) | copy-start | bytes 9437188
  87.8 4.5 %copy-start.3 = (bf16[512,2048]{1,0:T(8,128)(2,1)S(1)}, bf16[512,2048]{1,0:T(8,128)(2,1)}, u32[]{:S(2)}) copy-start(bf16[512,2048]{1,0:T(8,128)(2,1)} %get-tuple-element.14) | copy-start | bytes 6291460
  87.8 4.5 %copy-start.5 = (bf16[512,768]{1,0:T(8,128)(2,1)S(1)}, bf16[512,768]{1,0:T(8,128)(2,1)}, u32[]{:S(2)}) copy-start(bf16[512,768]{1,0:T(8,128)(2,1)} %param.9) | copy-start | bytes 2359300
  92.3 2.1 %copy-start.2 = (bf16[2048,768]{1,0:T(8,128)(2,1)S(1)}, bf16[2048,768]{1,0:T(8,128)(2,1)}, u32[]{:S(2)}) copy-start(bf16[2048,768]{1,0:T(8,128)(2,1)} %get-tuple-element.12) | copy-start | bytes 9437188
  92.3 2.5 %copy-start.4 = (bf16[512,2048]{1,0:T(8,128)(2,1)S(1)}, bf16[512,2048]{1,0:T(8,128)(2,1)}, u32[]{:S(2)}) copy-start(bf16[512,2048]{1,0:T(8,128)(2,1)} %get-tuple-element.11) | copy-start | bytes 6291460
  197.6 4.0 %copy-start = (f32[256,768]{1,0:T(8,128)S(1)}, f32[256,768]{1,0:T(8,128)}, u32[]{:S(2)}) copy-start(f32[256,768]{1,0:T(8,128)} %get-tuple-element.25) | copy-start | bytes 2359300

commit v2 on v0

v2 whole, which is shorter than its diff:
```python
import functools

import jax
import jax.numpy as jnp
from jax import lax
from jax.experimental import pallas as pl
from jax.experimental.pallas import tpu as pltpu
from jax.sharding import PartitionSpec as P

MESH = pl.DeviceIdType.MESH
F32 = jnp.float32
BF16 = jnp.bfloat16


def place(fs_count):
    fs, tp = lax.axis_index("fs"), lax.axis_index("tp")
    return lax.div(fs, 2), lax.rem(fs, 2), tp, fs_count // 2


def bits_of(tp_count):
    return [1 << b for b in range(tp_count.bit_length() - 1)]


def flip(tp, bit):
    return jnp.where(lax.rem(lax.div(tp, bit), 2) == 0, tp + bit, tp - bit)


def flips(tp, mask, bits):
    for bit in bits:
        if mask & bit:
            tp = flip(tp, bit)
    return tp


class Copies:
    def __init__(self, send_sem, recv_sem):
        self.send_sem, self.recv_sem = send_sem, recv_sem
        self.index, self.sent = {}, []

    def number(self, key):
        return self.index.setdefault(key, len(self.index))

    def make(self, key, src, dst, device):
        at = self.number(key) if isinstance(key, tuple) else key
        return pltpu.make_async_remote_copy(
            src_ref=src, dst_ref=dst, send_sem=self.send_sem.at[at], recv_sem=self.recv_sem.at[at],
            device_id=device, device_id_type=MESH,
        )

    def start(self, key, src, dst, device, when=None):
        copy = self.make(key, src, dst, device)
        self.sent.append((copy, when))
        under(when, copy.start)

    def arrived(self, key, dst, device):
        self.make(key, dst, dst, device).wait_recv()

    def drain(self):
        for copy, when in self.sent:
            under(when, copy.wait_send)


def under(when, action):
    if when is None:
        action()
    else:
        pl.when(when)(action)


def neighbours(z, x, tp, n, bits):
    up = (jnp.minimum(z + 1, n - 1) * 2 + x, tp)
    down = (jnp.maximum(z - 1, 0) * 2 + x, tp)
    beside = (z * 2 + 1 - x, tp)
    barrier = pltpu.get_barrier_semaphore()

    def greet(device):
        pl.semaphore_signal(barrier, inc=1, device_id=device, device_id_type=MESH)

    pl.when(z < n - 1)(lambda: greet(up))
    pl.when(z > 0)(lambda: greet(down))
    for device in [beside] + [(z * 2 + x, flip(tp, bit)) for bit in bits]:
        greet(device)
    ends = jnp.where(z < n - 1, 1, 0) + jnp.where(z > 0, 1, 0)
    pl.semaphore_wait(barrier, 1 + len(bits) + ends)
    return up, down, beside


def gather_kernel(fs_count, tp_count, early, xl, xe, w, out_xl, out_xe, out_w, ssem, rsem):
    z, x, tp, n = place(fs_count)
    bits = bits_of(tp_count)
    rows, cols = w.shape
    tokens = xl.shape[0]
    up, down, beside = neighbours(z, x, tp, n, bits)
    copies = Copies(ssem, rsem)
    first = pl.ds(0, early)
    size = (cols - early) // 256 * 128
    parts = (pl.ds(early, size), pl.ds(early + size, cols - early - size))

    def chunk(at, side):
        return pl.ds(pl.multiple_of((at * 2 + side) * rows, rows), rows)

    def pair(at):
        return pl.ds(pl.multiple_of(at * 2 * rows, 2 * rows), 2 * rows)

    def own_tokens(mask):
        return pl.ds(pl.multiple_of(flips(tp, mask, bits) * tokens, tokens), tokens)

    ways = (("u", up, z < n - 1), ("d", down, z > 0))
    mine = chunk(z, x)
    copies.start(("first",), w.at[:, first], out_w.at[mine, first], beside)
    for index, rest in enumerate(parts):
        for name, device, when in ways:
            copies.start((name, 0, index), w.at[:, rest], out_w.at[mine, rest], device, when)
    for name, src, out in (("e", xe, out_xe), ("l", xl, out_xl)):
        for bit in bits[::-1]:
            copies.start((name, bit, 0), src, out.at[own_tokens(0)], (z * 2 + x, flip(tp, bit)))
    for index, rest in enumerate(parts):
        copies.start(("beside", index), w.at[:, rest], out_w.at[mine, rest], beside)
    out_w[mine, :] = w[...]
    out_xe[own_tokens(0), :] = xe[...]
    out_xl[own_tokens(0), :] = xl[...]

    def origin(name, step):
        at = z - 1 - step if name == "u" else z + 1 + step
        has = at >= 0 if name == "u" else at <= n - 1
        return jnp.clip(at, 0, n - 1), has

    sides = []
    for step in range(n - 1):
        for index, rest in enumerate(parts):
            for name, device, when in ways:
                at, has = origin(name, step)
                ref = out_w.at[chunk(at, x), rest]
                pl.when(has)(lambda: copies.arrived((name, step, index), ref, device))
                copies.start((name, step + 1, index), ref, ref, device, has & when)
                copies.start(("beside", name, step, index), ref, ref, beside, has)
                sides.append((("beside", name, step, index), out_w.at[chunk(at, 1 - x), rest], has))
        if step == 0:
            theirs = out_w.at[chunk(z, 1 - x), first]
            copies.arrived(("first",), theirs, beside)
            both = out_w.at[pair(z), first]
            for name, device, when in ways:
                copies.start(("pair" + name, 0), both, both, device, when)
            for level, bit in enumerate(bits[::-1]):
                for mask in range(1, tp_count):
                    top = mask & -mask
                    if top > bit:
                        for out, key in ((out_xe, "e"), (out_xl, "l")):
                            ref = out.at[own_tokens(mask)]
                            if top == bit * 2:
                                copies.arrived((key, top, mask ^ top), ref, beside)
                            copies.start((key, bit, mask), ref, ref, (z * 2 + x, flip(tp, bit)))
    for step in range(n - 1):
        for name, device, when in ways:
            at, has = origin(name, step)
            ref = out_w.at[pair(at), first]
            pl.when(has)(lambda: copies.arrived(("pair" + name, step), ref, device))
            copies.start(("pair" + name, step + 1), ref, ref, device, has & when)
    for index, rest in enumerate(parts):
        copies.arrived(("beside", index), out_w.at[chunk(z, 1 - x), rest], beside)
    for key, ref, has in sides:
        pl.when(has)(lambda: copies.arrived(key, ref, beside))
    for out, key in ((out_xe, "e"), (out_xl, "l")):
        for mask in range(1, tp_count):
            if mask & 1:
                copies.arrived((key, 1, mask ^ 1), out.at[own_tokens(mask)], beside)
    copies.drain()


def add(a, b):
    return a.astype(F32) + b.astype(F32)


def reduce_kernel(
    fs_count, tp_count, early, dw, dx, gs, us, out_g, out_u, out_x,
    slots_p, last, slots_b, slots_z, slots_x, ssem, rsem,
):
    z, x, tp, n = place(fs_count)
    bits = bits_of(tp_count)
    rows, cols = gs.shape
    tokens = out_x.shape[0]
    up, down, beside = neighbours(z, x, tp, n, bits)
    copies = Copies(ssem, rsem)
    first, rest = pl.ds(0, early), pl.ds(early, 2 * cols - early)

    def chunk(at, side):
        return pl.ds(pl.multiple_of((at * 2 + side) * rows, rows), rows)

    def tp_chunk(mask):
        return pl.ds(pl.multiple_of(flips(tp, mask, bits) * tokens, tokens), tokens)

    near = jnp.where(z < n // 2, 0, 1)

    def way(d):
        to, back = z + 1 - 2 * d, z - 1 + 2 * d
        return d, (jnp.clip(to, 0, n - 1) * 2 + x, tp), (back >= 0) & (back <= n - 1)

    ways = (way(near), way(1 - near))

    def target_of(d, step):
        target = jnp.where(d == 0, n - 1 - step, step)
        return target, (1 - 2 * d) * (target - z) > 0

    def hop(name, d, step):
        return bases[name] + d * (n - 1) + step

    for k in range(n):
        copies.number(("b", k))
    bases = {}
    for name in "pz":
        bases[name] = len(copies.index)
        for k in range(2 * (n - 1)):
            copies.number((name, k))

    def pairs(step):
        for d, device, from_behind in ways:
            target, passes = target_of(d, step)
            own = dw.at[pl.ds(pl.multiple_of(target * 2 * rows, 2 * rows), 2 * rows), first]
            slot = slots_p.at[d, step]

            def pass_on(own=own, slot=slot, key=hop("p", d, step), device=device):
                copies.arrived(key, slot, device)
                slot[...] = add(slot[...], own[...]).astype(BF16)

            pl.when(passes & from_behind)(pass_on)
            copies.start(hop("p", d, step), slot, slot, device, passes & from_behind)
            start = copies.make(hop("p", d, step), own, slot, device)
            edge = passes & jnp.logical_not(from_behind)
            pl.when(edge)(start.start)
            edges.append((start, edge))

    edges = []
    for k in range(n):
        low = n - 1 - k
        low = jnp.where(low <= z, low - 1, low)
        high = jnp.where(k >= z, k + 1, k)
        at = z if k == n - 1 else jnp.where(z < n // 2, low, high)
        at = jnp.clip(at, 0, n - 1)
        copies.start(at, dw.at[chunk(at, 1 - x), rest], slots_b.at[at], beside)
    pairs(0)

    def above(bit):
        return [m for m in range(0, tp_count, 2 * bit)]

    slot_of = {}
    for bit in bits:
        for mask in above(bit):
            slot_of[bit, mask] = len(slot_of)

    def send_x(bit, mask, src):
        copies.start(("x", bit, mask), src, slots_x.at[slot_of[bit, mask]], (z * 2 + x, flip(tp, bit)))

    def recv_x(bit, mask):
        copies.arrived(("x", bit, mask), slots_x.at[slot_of[bit, mask]], beside)

    def sum_x(bit, mask):
        total = dx[tp_chunk(mask), :].astype(F32)
        for b in bits:
            if b <= bit:
                total = total + slots_x[slot_of[b, mask]].astype(F32)
        return total

    for mask in above(bits[0])[::-1]:
        send_x(bits[0], mask, dx.at[tp_chunk(mask | bits[0])])
    for step in range(1, n - 1):
        pairs(step)
    for level in range(1, len(bits)):
        bit, before = bits[level], bits[level - 1]
        for mask in above(bit)[::-1]:
            sent = mask | bit
            recv_x(before, sent)
            slot = slots_x.at[slot_of[before, sent]]
            slot[...] = sum_x(before, sent).astype(BF16)
            send_x(bit, mask, slot)

    def beside_sum(target):
        copies.arrived(target, slots_b.at[target], beside)
        slots_b[target] = add(slots_b[target], dw[chunk(target, x), rest]).astype(BF16)

    def chunks(step):
        for d, device, from_behind in ways:
            target, passes = target_of(d, step)
            slot = slots_z.at[d, step]

            def pass_on(slot=slot, key=hop("z", d, step), device=device, target=target):
                copies.arrived(key, slot, device)
                slot[...] = add(slot[...], slots_b[target]).astype(BF16)

            pl.when(passes)(lambda: beside_sum(target))
            pl.when(passes & from_behind)(pass_on)
            copies.start(hop("z", d, step), slot, slot, device, passes & from_behind)
            start = copies.make(hop("z", d, step), slots_b.at[target], slot, device)
            edge = passes & jnp.logical_not(from_behind)
            pl.when(edge)(start.start)
            edges.append((start, edge))

    chunks(0)
    theirs = pl.ds(pl.multiple_of((1 - x) * rows, rows), rows)
    ours = pl.ds(pl.multiple_of(x * rows, rows), rows)
    own_pair = dw.at[pl.ds(pl.multiple_of(z * 2 * rows, 2 * rows), 2 * rows), first]
    last[...] = own_pair[...].astype(F32)
    for d, from_behind in ((0, z > 0), (1, z < n - 1)):
        for step in range(n - 1):
            target = n - 1 - step if d == 0 else step

            def take(d=d, step=step):
                copies.arrived(hop("p", d, step), slots_p.at[d, step], beside)
                last[...] = last[...] + slots_p[d, step].astype(F32)

            pl.when((z == target) & from_behind)(take)
    slots_p[0, n - 1] = last[...].astype(BF16)
    copies.start(("last",), slots_p.at[0, n - 1, theirs, :], slots_p.at[1, n - 1, pl.ds(0, rows), :], beside)
    for step in range(1, n - 1):
        chunks(step)
    for b in bits:
        recv_x(b, 0)
    out_x[...] = sum_x(bits[-1], 0).astype(BF16)
    copies.arrived(z, slots_b.at[z], beside)
    left, right = pl.ds(0, cols - early), pl.ds(cols - early, cols)
    tail = pl.ds(early, cols - early)
    whole = add(slots_b[z], dw[chunk(z, x), rest])
    out_g[:, tail] = gs[:, tail] + whole[:, : cols - early]
    out_u[...] = us[...] + whole[:, cols - early :]
    copies.arrived(("last",), slots_p.at[1, n - 1, pl.ds(0, rows), :], beside)
    out_g[:, first] = gs[:, first] + (last[ours, :] + slots_p[1, n - 1, pl.ds(0, rows), :].astype(F32))
    for d, from_behind in ((0, z > 0), (1, z < n - 1)):
        for step in range(n - 1):
            target = n - 1 - step if d == 0 else step

            def take(d=d, step=step):
                slot = slots_z.at[d, step]
                copies.arrived(hop("z", d, step), slot, beside)
                out_g[:, tail] += slot[:, left].astype(F32)
                out_u[...] += slot[:, right].astype(F32)

            pl.when((z == target) & from_behind)(take)
    copies.sent += edges
    copies.drain()


def vmem(count):
    return [pl.BlockSpec(memory_space=pltpu.VMEM)] * count


def local(fs_count, tp_count, x_late, x_early, d_hidden, w_gate, w_up, gate_sum, up_sum):
    n = fs_count // 2
    tokens, width = x_early.shape
    rows, cols = w_gate.shape
    early = max(128, cols // 3 // 128 * 128)
    full = jax.ShapeDtypeStruct((fs_count * rows, 2 * cols), BF16)
    group = jax.ShapeDtypeStruct((tp_count * tokens, width), BF16)
    weights = jnp.concatenate([w_gate, w_up], axis=1)
    count = 2 * (tp_count - 1) + 10 * n + 3
    rows_late, rows_early, full_w = pl.pallas_call(
        functools.partial(gather_kernel, fs_count, tp_count, early),
        out_shape=(group, group, full),
        in_specs=vmem(3),
        out_specs=tuple(vmem(3)),
        scratch_shapes=[pltpu.SemaphoreType.DMA((count,)), pltpu.SemaphoreType.DMA((count,))],
        compiler_params=pltpu.CompilerParams(collective_id=0, has_side_effects=True),
        name="gather",
    )(x_late, x_early, weights)

    contract = (((1,), (1,)), ((), ()))
    tokens_dim = (((0,), (0,)), ((), ()))
    pre = jnp.dot(rows_early, full_w, preferred_element_type=F32)
    gate_early, up_early = pre[:, :cols], pre[:, cols:]
    s = jax.nn.sigmoid(gate_early)
    cotangent = d_hidden.astype(F32)
    d_gate = (cotangent * up_early * s * (1.0 + gate_early * (1.0 - s))).astype(BF16)
    d_up = (cotangent * gate_early * s).astype(BF16)
    d_both = jnp.concatenate([d_gate, d_up], axis=1)
    grad_w = lax.dot_general(rows_early, d_both, tokens_dim, preferred_element_type=F32).astype(BF16)
    partial_value = lax.dot_general(d_both, full_w, contract, preferred_element_type=F32).astype(BF16)
    pre = jnp.dot(rows_late, full_w, preferred_element_type=F32)
    gate_late, up_late = pre[:, :cols], pre[:, cols:]
    hidden_late = (gate_late * jax.nn.sigmoid(gate_late) * up_late).astype(BF16)

    count = (tp_count - 1) + 4 * (n - 1) + n + 1
    gate_out, up_out, grad_input = pl.pallas_call(
        functools.partial(reduce_kernel, fs_count, tp_count, early),
        out_shape=(
            jax.ShapeDtypeStruct(gate_sum.shape, F32),
            jax.ShapeDtypeStruct(up_sum.shape, F32),
            jax.ShapeDtypeStruct(x_early.shape, BF16),
        ),
        in_specs=vmem(4),
        out_specs=tuple(vmem(3)),
        scratch_shapes=[
            pltpu.VMEM((2, n, 2 * rows, early), BF16),
            pltpu.VMEM((2 * rows, early), F32),
            pltpu.VMEM((n, rows, 2 * cols - early), BF16),
            pltpu.VMEM((2, n - 1, rows, 2 * cols - early), BF16),
            pltpu.VMEM((tp_count - 1, tokens, width), BF16),
            pltpu.SemaphoreType.DMA((count,)),
            pltpu.SemaphoreType.DMA((count,)),
        ],
        compiler_params=pltpu.CompilerParams(collective_id=1, has_side_effects=True),
        name="reduce",
    )(grad_w, partial_value, gate_sum, up_sum)
    return (hidden_late, grad_input, gate_out, up_out)


def solution(mesh):
    return jax.shard_map(
        functools.partial(local, mesh.shape["fs"], mesh.shape["tp"]),
        mesh=mesh,
        in_specs=(
            P(("fs", "tp"), None),
            P(("fs", "tp"), None),
            P("fs", "tp"),
            P("fs", "tp"),
            P("fs", "tp"),
            P("fs", "tp"),
            P("fs", "tp"),
        ),
        out_specs=(P("fs", "tp"), P(("fs", "tp"), None), P("fs", "tp"), P("fs", "tp")),
        check_vma=False,
    )
```

time: 445 us -> 170 us (0.38)
  waiting for transfers between devices: 384 us -> 0 us
  Pallas kernels: 0 us -> 139 us
  between operations: 14.2 us -> 0.7 us
  matrix products: 29.6 us -> 19.9 us
  local copies, waits for them, and re-layouts: 13 us -> 5.42 us
    reduce_scatter x2 -> x0, waiting for transfers between devices: 226 us -> none  [the longest x1 196 us: local(): lax.psum_scatter(lax.dot_general(rows_early, d_both, tokens_dim, preferre...]
    all_gather x4 -> x0, waiting for transfers between devices: 156 us -> none  [the longest x1 59.1 us: local(): lax.all_gather(w_up, 'fs', axis=0, tiled=True)]
    pallas_call x0 -> x2, Pallas kernels: none -> 139 us  [the longest x1 70.3 us: local(): pl.pallas_call(functools.partial(gather_kernel, fs_count, tp_count, early...]
    dot_general x5 -> x4, matrix products: 29.6 us -> 19.9 us  [the longest x1 6.31 us: local(): pre = jnp.dot(rows_late, full_w, preferred_element_type=F32)]
    unnamed x15 -> x11, local copies, waits for them, and re-layouts: 9.85 us -> 5.42 us
  transfers between devices with their start and end apart: 6 -> 0, of which waited for: 6 -> 0; matrix products, arithmetic and copies ran while one was open for 7% -> 0% of each run, Pallas kernels for 0% -> 0%
where the time goes in v2:
time: 170 us; the launch traced here: 169 us
  Pallas kernels  139 us (82%)
  matrix products  19.9 us (12%)
  local copies, waits for them, and re-layouts  5.42 us (3%)
  other arithmetic  4.16 us (2%)
    pallas_call x1, Pallas kernels, local(): pl.pallas_call(functools.partial(gather_kernel, fs_count, tp_count, early...  70.3 us
    pallas_call x1, Pallas kernels, local(): pl.pallas_call(functools.partial(reduce_kernel, fs_count, tp_count, early...  68.8 us
    dot_general x1, matrix products, local(): pre = jnp.dot(rows_late, full_w, preferred_element_type=F32)  6.31 us
    dot_general x1, matrix products, local(): lax.dot_general(rows_early, d_both, tokens_dim, preferred_element_type=F32)  5.53 us
    unnamed x11, local copies, waits for them, and re-layouts  5.42 us
    dot_general x1, matrix products, local(): lax.dot_general(d_both, full_w, contract, preferred_element_type=F32)  4.7 us
    dot_general x1, matrix products, local(): pre = jnp.dot(rows_early, full_w, preferred_element_type=F32)  3.4 us

profile of v2, /device:TPU:0, one launch (start us, length us, event | category | flops | bytes accessed | tf_op | source)
XLA Modules:
  0.0 169.3 jit_solution(5894845353179513231)
XLA Ops:
  0.6 2.0 %pad_maximum_fusion.3.w = bf16[256,1536]{1,0:T(8,128)(2,1)} fusion(bf16[256,768]{1,0:T(8,128)(2,1)} %param.11, bf16[256,768]{1,0:T(8,128)(2,1)} %param.10), kind=kLoop, calls=%fused_computation.13 | loop fusion | flops 1572864 | bytes 1572864 | tf_op jit(solution)/shard_map/concatenate | solution.py:352
  2.7 70.3 %gather.1 = (bf16[512,2048]{1,0:T(8,128)(2,1)}, bf16[512,2048]{1,0:T(8,128)(2,1)}, bf16[2048,1536]{1,0:T(8,128)(2,1)}) custom-call(bf16[128,2048]{1,0:T(8,128)(2,1)} %xl.1, bf16[128,2048]{1,0:T(8,128)(2,1)} %xe.1, bf16[256,1536]{1,0:T(8,128)(2,1)} %pad_maximum_fusion.3.w), custom_call_target="tpu_custom_call" | custom-call | tf_op jit(solution)/shard_map/gather/pallas_call | solution.py:354
  73.0 0.0 copy-start.2
  73.0 6.3 %fusion.8 = f32[512,1536]{1,0:T(8,128)S(1)} fusion(bf16[512,2048]{1,0:T(8,128)(2,1)} %get-tuple-element.10, bf16[2048,1536]{1,0:T(8,128)(2,1)} %get-tuple-element.11), kind=kOutput, calls=%fused_computation.16 | convolution fusion | flops 3221225472 | bytes 11534336 | tf_op jit(solution)/shard_map/dot_general | solution.py:375
  79.3 0.0 copy-start.3
  79.4 1.4 fusion.5
  80.7 0.0 copy-done.2
  80.7 0.5 copy-done.3
  81.2 0.0 copy-start.1
  81.2 3.4 %fusion.9 = f32[512,1536]{1,0:T(8,128)S(1)} fusion(bf16[512,2048]{1,0:T(8,128)(2,1)S(1)} %copy-done.3, bf16[2048,1536]{1,0:T(8,128)(2,1)S(1)} %copy-done.2), kind=kOutput, calls=%fused_computation.17 | convolution fusion | flops 3221225472 | bytes 11534336 | tf_op jit(solution)/shard_map/dot_general | solution.py:366
  84.6 0.0 copy-done.1
  84.6 0.8 fusion.2
  85.4 4.7 %convolution_convert_fusion.1.dx = bf16[512,2048]{1,0:T(8,128)(2,1)} fusion(bf16[2048,1536]{1,0:T(8,128)(2,1)S(1)} %copy-done.2, bf16[512,768]{1,0:T(8,128)(2,1)S(1)} %get-tuple-element.17, bf16[512,768]{1,0:T(8,128)(2,1)S(1)} %get-tuple-element.16), kind=kOutput, calls=%fused_computation.1 | convolution fusion | flops 3225419776 | bytes 9961472 | tf_op jit(solution)/shard_map/dot_general | solution.py:374
  90.1 5.5 %convolution_convert_fusion.dw = bf16[2048,1536]{1,0:T(8,128)(2,1)} fusion(bf16[512,2048]{1,0:T(8,128)(2,1)S(1)} %copy-done.3, bf16[512,768]{1,0:T(8,128)(2,1)S(1)} %get-tuple-element.17, bf16[512,768]{1,0:T(8,128)(2,1)S(1)} %get-tuple-element.16), kind=kOutput, calls=%fused_computation | convolution fusion | flops 3227516928 | bytes 9961472 | tf_op jit(solution)/shard_map/dot_general | solution.py:373
  95.6 68.8 %reduce.1 = (f32[256,768]{1,0:T(8,128)}, f32[256,768]{1,0:T(8,128)}, bf16[128,2048]{1,0:T(8,128)(2,1)}) custom-call(bf16[2048,1536]{1,0:T(8,128)(2,1)} %convolution_convert_fusion.dw, bf16[512,2048]{1,0:T(8,128)(2,1)} %convolution_convert_fusion.1.dx, f32[256,768]{1,0:T(8,128)} %gs.1, f32[256,768]{1,0:T(8,128)} %us.1), custom_call_target="tpu_custom_call" | custom-call | tf_op jit(solution)/shard_map/reduce/pallas_call | solution.py:380
  164.4 0.0 copy-start
  164.4 2.0 %copy.14 = bf16[128,2048]{1,0:T(8,128)(2,1)} copy(bf16[128,2048]{1,0:T(8,128)(2,1)} %get-tuple-element.23) | data formatting | bytes 1048576
  166.4 2.1 %copy.15 = f32[256,768]{1,0:T(8,128)} copy(f32[256,768]{1,0:T(8,128)} %get-tuple-element.24) | data formatting | bytes 1572864
  168.5 0.0 copy-done
  168.5 0.9 copy.16
Async XLA Ops:
  73.0 7.7 %copy-start.2 = (bf16[2048,1536]{1,0:T(8,128)(2,1)S(1)}, bf16[2048,1536]{1,0:T(8,128)(2,1)}, u32[]{:S(2)}) copy-start(bf16[2048,1536]{1,0:T(8,128)(2,1)} %get-tuple-element.11) | copy-start | bytes 18874372
  79.3 1.9 %copy-start.3 = (bf16[512,2048]{1,0:T(8,128)(2,1)S(1)}, bf16[512,2048]{1,0:T(8,128)(2,1)}, u32[]{:S(2)}) copy-start(bf16[512,2048]{1,0:T(8,128)(2,1)} %get-tuple-element.12) | copy-start | bytes 6291460
  81.2 3.4 %copy-start.1 = (bf16[512,768]{1,0:T(8,128)(2,1)S(1)}, bf16[512,768]{1,0:T(8,128)(2,1)}, u32[]{:S(2)}) copy-start(bf16[512,768]{1,0:T(8,128)(2,1)} %param.9) | copy-start | bytes 2359300
  164.4 4.0 %copy-start = (f32[256,768]{1,0:T(8,128)S(1)}, f32[256,768]{1,0:T(8,128)}, u32[]{:S(2)}) copy-start(f32[256,768]{1,0:T(8,128)} %get-tuple-element.25) | copy-start | bytes 2359300
